TPU v7x, 32 devices: a whole 2x2x4 slice. The times are simulated.
32 devices in a mesh: sp: 8 (over z, y), tp: 4 (over x, core).
Axes of the slice: x: 2, y: 2, z: 4, core: 2. Of those that a mesh axis runs over, the one named last changes fastest.
Arguments:
- stream: bfloat16 [8192, 4096], P('sp', 'tp'), may hold values from -11 to 11
- norm_gain: bfloat16 [3, 4096], P(None, 'tp'), may hold values from 0.099609375 to 1.8984375
- pool_weight: bfloat16 [3, 4, 1024, 1024], P(None, 'tp', 'sp'), may hold values from -0.1875 to 0.1875
- pool_scale: bfloat16 [3, 4096], P(None, 'tp'), may hold values from 0.099609375 to 1.8984375
Outputs:
- mixed: bfloat16 [8192, 4096], P('sp', 'tp')
All inputs are finite; a program needn't handle non-finite values.
Results may differ from a plain program's by a relative error of at most 0.015.
Values may be sent and summed in bfloat16 or wider, within the bound.
A program may use at most 64 MiB of HBM per device.

v0:
```python
import jax
import jax.numpy as jnp
from jax import lax
from jax.sharding import PartitionSpec as P

D = 4096
POOL_GROUPS = 4
norm_eps = 1e-06


def padded(value, sides, width):
    for axis, dim in sides:
        devices, length = (lax.axis_size(axis), value.shape[dim])
        up = [(i, (i + 1) % devices) for i in range(devices - 1)]
        down = [(j, i) for i, j in up]
        last = lax.slice_in_dim(value, length - width, length, axis=dim)
        initial = lax.slice_in_dim(value, 0, width, axis=dim)
        before = lax.ppermute(last, axis, up)
        after = lax.ppermute(initial, axis, down)
        value = jnp.concatenate([before, value, after], axis=dim)
    return value


def window_pool(extended, out_rows, centre, halves, seq_total, reach_rows, per_dev, group_width):
    ext_float = extended.astype(jnp.float32).reshape(extended.shape[0], per_dev, group_width)
    window_sums = jnp.zeros((out_rows, per_dev, group_width), jnp.float32)
    for offset in range(-reach_rows, reach_rows):
        in_window = ((offset >= -halves) & (offset < halves)).astype(jnp.float32)
        window_sums = (
            window_sums
            + ext_float[reach_rows + offset : reach_rows + offset + out_rows]
            * in_window[None, :, None]
        )
    low_end = jnp.maximum(centre[:, None] - halves[None, :], 0)
    high_end = jnp.minimum(centre[:, None] + halves[None, :], seq_total)
    counts = jnp.maximum(high_end - low_end, 1).astype(jnp.float32)
    middle = ext_float[reach_rows : reach_rows + out_rows]
    return (window_sums / counts[:, :, None] - middle).astype(jnp.bfloat16)


def local(stream, norm_gain, pool_weight, pool_scale):
    tok_rows, local_width = stream.shape
    layers, per_dev, shard_rows, group_width = pool_weight.shape
    reach_rows = 2**POOL_GROUPS // 2
    seq_total = tok_rows * lax.axis_size("sp")
    first_pos = lax.axis_index("sp") * tok_rows
    groups = lax.axis_index("tp") * per_dev + jnp.arange(per_dev, dtype=jnp.int32)
    halves = jnp.left_shift(jnp.int32(1), groups)
    deep_rows = reach_rows * layers
    current = padded(stream, (("sp", 0),), deep_rows)
    base_pos = first_pos - deep_rows
    for layer_idx in range(layers):
        ext_rows = current.shape[0]
        positions = base_pos + jnp.arange(ext_rows, dtype=jnp.int32)
        inside = (positions >= 0) & (positions < seq_total)
        current_f = current.astype(jnp.float32)
        square_sums = lax.psum(jnp.sum(current_f * current_f, axis=1), "tp")
        row_scale = lax.rsqrt(square_sums / D + norm_eps)
        normed = current_f * row_scale[:, None] * norm_gain[layer_idx].astype(jnp.float32)
        normed = jnp.where(inside[:, None], normed, 0.0).astype(jnp.bfloat16)
        out_rows = ext_rows - 2 * reach_rows
        residual = current_f[reach_rows : ext_rows - reach_rows]
        centre = positions[reach_rows : ext_rows - reach_rows]
        base_pos = base_pos + reach_rows
        pooled = window_pool(
            normed, out_rows, centre, halves, seq_total, reach_rows, per_dev, group_width
        )
        branch = jnp.einsum(
            "tgc,gcd->tgd",
            pooled,
            lax.all_gather(pool_weight[layer_idx], "sp", axis=1, tiled=True),
            preferred_element_type=jnp.float32,
        )
        branch = branch.reshape(out_rows, local_width)
        current = (residual + branch * pool_scale[layer_idx].astype(jnp.float32)).astype(
            jnp.bfloat16
        )
    return current


def solution(mesh):
    placed = (P("sp", "tp"), P(None, "tp"), P(None, "tp", "sp", None), P(None, "tp"))
    return jax.shard_map(
        local, mesh=mesh, in_specs=placed, out_specs=P("sp", "tp"), check_vma=False
    )
```

profile of v0, /device:TPU:0, one launch (start us, length us, event | category | flops | bytes accessed | tf_op | source)
XLA Modules:
  0.0 213.5 jit_solution(14513719529926578591)
XLA Ops:
  6.5 2.2 %fusion.70 = (bf16[1,1,128,1024]{3,2,1,0:T(8,128)(2,1)}, bf16[1,1,128,1024]{3,2,1,0:T(8,128)(2,1)}, bf16[1,1,128,1024]{3,2,1,0:T(8,128)(2,1)}) fusion(bf16[3,1,128,1024]{3,2,1,0:T(8,128)(2,1)} %param.6), kind=kLoop, calls=%fused_computation.141 | loop fusion | bytes 1572864 | tf_op jit(solution)/shard_map/slice | solution.py:71
  8.7 0.0 all-gather.9.cloned.1.call-start
  8.8 0.7 all-gather.9.cloned.1.call-update
  9.5 0.8 fusion.69
  10.4 4.9 %collective-permute-start = (bf16[24,1024]{1,0:T(8,128)(2,1)S(1)}, bf16[24,1024]{1,0:T(8,128)(2,1)S(1)}, u32[]{:S(2)}, u32[]{:S(2)}) collective-permute-start(bf16[24,1024]{1,0:T(8,128)(2,1)S(1)} %get-tuple-element.5), channel_id=1, source_target_pairs={{0,4},{4,8},{8,12},{12,16},{16,20},{20,24},{24,28},{1,5},{5,9},{9,... | collective-permute-start | bytes 147464 | tf_op jit(solution)/shard_map/ppermute | solution.py:18
  15.3 1.3 collective-permute-start.1
  16.6 0.8 slice_convert_fusion.1
  17.5 0.8 slice_convert_fusion
  18.3 0.1 maximum_convert_fusion.2
  18.4 0.1 maximum_convert_fusion.1
  18.5 0.1 maximum_convert_fusion.3
  18.7 2.5 %collective-permute-done.1 = bf16[24,1024]{1,0:T(8,128)(2,1)S(1)} collective-permute-done((bf16[24,1024]{1,0:T(8,128)(2,1)S(1)}, bf16[24,1024]{1,0:T(8,128)(2,1)S(1)}, u32[]{:S(2)}, u32[]{:S(2)}) %collective-permute-start.1) | collective-permute-done | bytes 49184 | tf_op jit(solution)/shard_map/ppermute | solution.py:19
  21.2 0.5 multiply_reduce_fusion
  21.8 6.2 %psum.21 = f32[1072]{0:T(1024)S(1)} all-reduce(f32[1072]{0:T(1024)S(1)} %multiply_reduce_fusion), channel_id=1, replica_groups=mesh['sp'=8,'tp'=4] {'tp'}, use_global_device_ids=true, to_apply=%region_1.0 | all-reduce | flops 1072 | bytes 8576 | tf_op jit(solution)/shard_map/psum | solution.py:57
  27.9 2.5 %maximum_convert_fusion = f32[1072,1024]{1,0:T(8,128)} fusion(bf16[24,1024]{1,0:T(8,128)(2,1)S(1)} %collective-permute-done.1, bf16[1024,1024]{1,0:T(8,128)(2,1)S(1)} %copy-done, bf16[24,1024]{1,0:T(8,128)(2,1)S(1)} %collective-permute-done), kind=kLoop, calls=%fused_computation.115 | loop fusion | flops 6586368 | bytes 6586368 | tf_op jit(solution)/shard_map/convert_element_type | solution.py:56
  30.5 2.9 %fusion.59 = f32[1072,1024]{1,0:T(8,128)} fusion(f32[1024]{0:T(1024)S(1)} %bitcast.21, f32[1072]{0:T(1024)S(1)} %add_rsqrt_fusion.2, pred[1072]{0:T(1024)(128)(4,1)S(1)} %compare_and_fusion.2, bf16[24,1024]{1,0:T(8,128)(2,1)S(1)} %collective-permute-done.1, bf16[1024,1024]{1,0:T(8,128)(2,1)S(1)} %copy-done, bf16[24,1024]{1,0:T(8,128)(2,1)S(1)} %collective-permute-done), kind=kLoop, calls=%fused_computation.114 | loop fusion | flops 12075008 | bytes 6595824 | tf_op jit(solution)/shard_map/convert_element_type | solution.py:25
  33.4 28.0 %all-gather.7.cloned.1.call-done = bf16[1,1,1024,1024]{3,2,1,0:T(8,128)(2,1)} async-done(((bf16[1,1,128,1024]{3,2,1,0:T(8,128)(2,1)}), bf16[1,1,1024,1024]{3,2,1,0:T(8,128)(2,1)}) %all-gather.7.cloned.1.call-update) | async-done | bytes 2097168 | tf_op jit(solution)/shard_map/all_gather | solution.py:71
  61.4 42.3 %multiply_reduce_fusion.1 = (f32[1056]{0:T(1024)S(1)}, f32[1056,1024]{1,0:T(8,128)}) fusion(f32[1024]{0:T(1024)S(1)} %bitcast.24, bf16[1,1,1024,1024]{3,2,1,0:T(8,128)(2,1)} %all-gather.7.cloned.1.call-done, f32[1072,1024]{1,0:T(8,128)} %fusion.59, f32[1056]{0:T(1024)S(1)} %maximum_convert_fusion.2, f32[]{:T(128)S(6)} %mul.631, f32[]{:T(128)S(6)} %mul.628, ...), kind=kOutput, calls=%fused_computation.40 | convolution fusion | flops 2257845248 | bytes 79966528 | tf_op jit(solution)/shard_map/tgc,gcd->tgd/dot_general | solution.py:68
  103.7 6.3 %psum.22 = f32[1056]{0:T(1024)S(1)} all-reduce(f32[1056]{0:T(1024)S(1)} %get-tuple-element.16), channel_id=1, replica_groups=mesh['sp'=8,'tp'=4] {'tp'}, use_global_device_ids=true, to_apply=%region_3.4 | all-reduce | flops 1056 | bytes 8448 | tf_op jit(solution)/shard_map/psum | solution.py:57
  110.0 4.7 %fusion.60 = f32[1056,1024]{1,0:T(8,128)} fusion(f32[1056,1024]{1,0:T(8,128)} %get-tuple-element.17, f32[1024]{0:T(1024)S(1)} %bitcast.20, f32[1056]{0:T(1024)S(1)} %add_rsqrt_fusion.1, pred[1056]{0:T(1024)(128)(4,1)S(1)} %compare_and_fusion.1), kind=kLoop, calls=%fused_computation.116 | loop fusion | flops 5406720 | bytes 8660128 | tf_op jit(solution)/shard_map/convert_element_type | solution.py:25
  114.8 41.7 %multiply_reduce_fusion.2 = (f32[1040]{0:T(1024)S(1)}, f32[1040,1024]{1,0:T(8,128)}) fusion(f32[1024]{0:T(1024)S(1)} %bitcast.23, bf16[1,1,1024,1024]{3,2,1,0:T(8,128)(2,1)} %all-gather.9.cloned.1.call-done, f32[1056,1024]{1,0:T(8,128)} %fusion.60, f32[1040]{0:T(1024)S(1)} %maximum_convert_fusion.1, f32[]{:T(128)S(6)} %mul.631, f32[]{:T(128)S(6)} %mul.628, ...), kind=kOutput, calls=%fused_computation.75 | convolution fusion | flops 2223635456 | bytes 78786752 | tf_op jit(solution)/shard_map/tgc,gcd->tgd/dot_general | solution.py:68
  156.4 6.7 %psum.23 = f32[1040]{0:T(1024)S(1)} all-reduce(f32[1040]{0:T(1024)S(1)} %get-tuple-element.18), channel_id=1, replica_groups=mesh['sp'=8,'tp'=4] {'tp'}, use_global_device_ids=true, to_apply=%region_5.6 | all-reduce | flops 1040 | bytes 8320 | tf_op jit(solution)/shard_map/psum | solution.py:57
  163.1 4.7 %fusion.63 = f32[1040,1024]{1,0:T(8,128)} fusion(f32[1040,1024]{1,0:T(8,128)} %get-tuple-element.19, f32[1024]{0:T(1024)S(1)} %bitcast.19, f32[1040]{0:T(1024)S(1)} %add_rsqrt_fusion, pred[1040]{0:T(1024)(128)(4,1)S(1)} %compare_and_fusion), kind=kLoop, calls=%fused_computation.118 | loop fusion | flops 5324800 | bytes 8528976 | tf_op jit(solution)/shard_map/convert_element_type | solution.py:25
  167.8 39.2 %fusion.55 = bf16[1024,1024]{1,0:T(8,128)(2,1)} fusion(f32[1040,1024]{1,0:T(8,128)} %get-tuple-element.19, bf16[1,1,1024,1024]{3,2,1,0:T(8,128)(2,1)} %all-gather.11.cloned.1.call-done, f32[1024]{0:T(1024)S(1)} %bitcast.22, f32[1040,1024]{1,0:T(8,128)} %fusion.63, f32[1024]{0:T(1024)S(1)} %maximum_convert_fusion.3, f32[]{:T(128)S(6)} %mul.631, ...), kind=kOutput, calls=%fused_computation.110 | convolution fusion | flops 2186280960 | bytes 75505728 | tf_op jit(solution)/shard_map/tgc,gcd->tgd/dot_general | solution.py:68
  (18 shorter events, 0.1 us)
Async XLA Ops:
  6.5 14.7 %copy-start = (bf16[1024,1024]{1,0:T(8,128)(2,1)S(1)}, bf16[1024,1024]{1,0:T(8,128)(2,1)}, u32[]{:S(2)}) copy-start(bf16[1024,1024]{1,0:T(8,128)(2,1)} %param.4) | copy-start | bytes 6291460
  6.5 54.9 %all-gather.7.cloned.1.call-start = ((), (), s32[]{:S(2)}) async-start(), calls=%async_computation | async-start | bytes 2359296 | tf_op jit(solution)/shard_map/all_gather | solution.py:71
  8.7 106.1 %all-gather.9.cloned.1.call-start = ((), (), s32[]{:S(2)}) async-start(), calls=%async_computation.1 | async-start | bytes 2359296 | tf_op jit(solution)/shard_map/all_gather | solution.py:71
  9.5 158.3 %all-gather.11.cloned.1.call-start = ((), (), s32[]{:S(2)}) async-start(), calls=%async_computation.2 | async-start | bytes 2359296 | tf_op jit(solution)/shard_map/all_gather | solution.py:71
  10.4 8.3 %collective-permute-start = (bf16[24,1024]{1,0:T(8,128)(2,1)S(1)}, bf16[24,1024]{1,0:T(8,128)(2,1)S(1)}, u32[]{:S(2)}, u32[]{:S(2)}) collective-permute-start(bf16[24,1024]{1,0:T(8,128)(2,1)S(1)} %get-tuple-element.5), channel_id=1, source_target_pairs={{0,4},{4,8},{8,12},{12,16},{16,20},{20,24},{24,28},{1,5},{5,9},{9,... | collective-permute-start | bytes 147464 | tf_op jit(solution)/shard_map/ppermute | solution.py:18
  15.3 6.0 %collective-permute-start.1 = (bf16[24,1024]{1,0:T(8,128)(2,1)S(1)}, bf16[24,1024]{1,0:T(8,128)(2,1)S(1)}, u32[]{:S(2)}, u32[]{:S(2)}) collective-permute-start(bf16[24,1024]{1,0:T(8,128)(2,1)S(1)} %get-tuple-element.6), channel_id=1, source_target_pairs={{4,0},{8,4},{12,8},{16,12},{20,16},{24,20},{28,24},{5,1},{9,5},{13... | collective-permute-start | bytes 147464 | tf_op jit(solution)/shard_map/ppermute | solution.py:19
Sparse Core Ops, SparseCore 0:
  9.5 51.8 all-gather.6
  63.5 47.6 all-gather.8
  113.3 47.6 all-gather.10
where the time goes:
time: 214 us
  matrix products  123 us (57%)
  waiting for transfers between devices  31.3 us (15%)
  blocking collectives  19.2 us (9%)
  other arithmetic  17.3 us (8%)
  between operations  13.4 us (6%)
  starting transfers between devices  6.26 us (3%)
  local copies, waits for them, and re-layouts  3 us (1%)
    dot_general x3, matrix products, local(): jnp.einsum('tgc,gcd->tgd', pooled, lax.all_gather(pool_weight[layer_idx],...  123 us
    all_gather x3, waiting for transfers between devices, local(): lax.all_gather(pool_weight[layer_idx], 'sp', axis=1, tiled=True)  28 us
    psum x3, blocking collectives, local(): square_sums = lax.psum(jnp.sum(current_f * current_f, axis=1), 'tp')  19.2 us
    convert_element_type x3, other arithmetic, window_pool(): extended.astype(jnp.float32)  12.3 us
    ppermute x1, starting transfers between devices, padded(): before = lax.ppermute(last, axis, up)  4.89 us
  transfers between devices with their start and end apart: 5, of which 2 were waited for; matrix products, arithmetic and copies ran while one was open for 48% of the time, Pallas kernels for 0%

commit v1 on v0

--- a/solution.py
+++ b/solution.py
@@ -54,7 +54,9 @@
         positions = base_pos + jnp.arange(ext_rows, dtype=jnp.int32)
         inside = (positions >= 0) & (positions < seq_total)
         current_f = current.astype(jnp.float32)
-        square_sums = lax.psum(jnp.sum(current_f * current_f, axis=1), "tp")
+        part = jnp.sum(current_f * current_f, axis=1)
+        parts = lax.all_gather(part, "tp", axis=0, tiled=False)
+        square_sums = parts.sum(axis=0)
         row_scale = lax.rsqrt(square_sums / D + norm_eps)
         normed = current_f * row_scale[:, None] * norm_gain[layer_idx].astype(jnp.float32)
         normed = jnp.where(inside[:, None], normed, 0.0).astype(jnp.bfloat16)

time: 214 us -> 223 us (1.042)
  blocking collectives: 19.2 us -> 32 us
  waiting for transfers between devices: 31.3 us -> 22.8 us
  local copies, waits for them, and re-layouts: 3 us -> 5.54 us
    unnamed x0 -> x3, blocking collectives: none -> 32 us
    psum x3 -> x0, blocking collectives: 19.2 us -> none  [local(): square_sums = lax.psum(jnp.sum(current_f * current_f, axis=1), 'tp')]
    all_gather x3, waiting for transfers between devices: 28 us -> 22 us  [local(): lax.all_gather(pool_weight[layer_idx], 'sp', axis=1, tiled=True)]
    ppermute x1, waiting for transfers between devices: 2.54 us -> 0.01 us  [padded(): after = lax.ppermute(initial, axis, down)]
    unnamed x2 -> x9, local copies, waits for them, and re-layouts: 0.01 us -> 2.3 us
  transfers between devices with their start and end apart: 5 -> 5, of which waited for: 2 -> 1; matrix products, arithmetic and copies ran while one was open for 48% -> 47% of each run, Pallas kernels for 0% -> 0%
where the time goes in v1:
time: 223 us; the launch traced here: 222 us
  matrix products  123 us (55%)
  blocking collectives  32 us (14%)
  waiting for transfers between devices  22.8 us (10%)
  other arithmetic  17.4 us (8%)
  between operations  15.4 us (7%)
  starting transfers between devices  6.26 us (3%)
  local copies, waits for them, and re-layouts  5.54 us (2%)
    dot_general x3, matrix products, local(): jnp.einsum('tgc,gcd->tgd', pooled, lax.all_gather(pool_weight[layer_idx],...  123 us
    unnamed x3, blocking collectives  32 us
    all_gather x3, waiting for transfers between devices, local(): lax.all_gather(pool_weight[layer_idx], 'sp', axis=1, tiled=True)  22 us
    convert_element_type x3, other arithmetic, window_pool(): extended.astype(jnp.float32)  12.3 us
    ppermute x1, starting transfers between devices, padded(): before = lax.ppermute(last, axis, up)  4.89 us
  transfers between devices with their start and end apart: 5, of which 1 were waited for; matrix products, arithmetic and copies ran while one was open for 47% of the time, Pallas kernels for 0%

profile of v1, /device:TPU:0, one launch (start us, length us, event | category | flops | bytes accessed | tf_op | source)
XLA Modules:
  0.0 222.4 jit_solution(346212120320951949)
XLA Ops:
  6.5 2.2 fusion.70
  8.8 0.7 all-gather.12.cloned.1.call-update
  9.5 0.8 fusion.69
  10.4 4.9 %collective-permute-start = (bf16[24,1024]{1,0:T(8,128)(2,1)S(1)}, bf16[24,1024]{1,0:T(8,128)(2,1)S(1)}, u32[]{:S(2)}, u32[]{:S(2)}) collective-permute-start(bf16[24,1024]{1,0:T(8,128)(2,1)S(1)} %get-tuple-element.5), channel_id=1, source_target_pairs={{0,4},{4,8},{8,12},{12,16},{16,20},{20,24},{24,28},{1,5},{5,9},{9,... | collective-permute-start | bytes 147464 | tf_op jit(solution)/shard_map/ppermute | solution.py:18
  15.3 1.3 collective-permute-start.1
  16.6 0.8 slice_convert_fusion.1
  17.5 0.8 slice_convert_fusion
  18.7 1.3 dynamic-slice
  22.0 0.5 multiply_reduce_fusion
  22.6 0.3 dynamic-update-slice
  22.9 10.9 %all-reduce = f32[4288]{0:T(1024)S(1)} all-reduce(f32[4288]{0:T(1024)S(1)} %dynamic-update-slice), channel_id=2, replica_groups=mesh['sp'=8,'tp'=4] {'tp'}, use_global_device_ids=true, to_apply=%add | all-reduce | flops 4288 | bytes 34304
  33.8 0.1 reshape.457
  33.9 2.6 %maximum_convert_fusion = f32[1072,1024]{1,0:T(8,128)} fusion(bf16[24,1024]{1,0:T(8,128)(2,1)S(1)} %collective-permute-done.1, bf16[1024,1024]{1,0:T(8,128)(2,1)S(1)} %copy-done, bf16[24,1024]{1,0:T(8,128)(2,1)S(1)} %collective-permute-done), kind=kLoop, calls=%fused_computation.115 | loop fusion | flops 6586368 | bytes 6586368 | tf_op jit(solution)/shard_map/convert_element_type | solution.py:56
  36.5 2.9 %fusion.59 = f32[1072,1024]{1,0:T(8,128)} fusion(f32[1024]{0:T(1024)S(1)} %bitcast.24, f32[1072]{0:T(1024)S(1)} %add_rsqrt_fusion.2, pred[1072]{0:T(1024)(128)(4,1)S(1)} %compare_and_fusion.2, bf16[24,1024]{1,0:T(8,128)(2,1)S(1)} %collective-permute-done.1, bf16[1024,1024]{1,0:T(8,128)(2,1)S(1)} %copy-done, bf16[24,1024]{1,0:T(8,128)(2,1)S(1)} %collective-permute-done), kind=kLoop, calls=%fused_computation.114 | loop fusion | flops 12075008 | bytes 6595824 | tf_op jit(solution)/shard_map/convert_element_type | solution.py:25
  39.4 22.0 %all-gather.10.cloned.1.call-done = bf16[1,1,1024,1024]{3,2,1,0:T(8,128)(2,1)} async-done(((bf16[1,1,128,1024]{3,2,1,0:T(8,128)(2,1)}), bf16[1,1,1024,1024]{3,2,1,0:T(8,128)(2,1)}) %all-gather.10.cloned.1.call-update) | async-done | bytes 2097168 | tf_op jit(solution)/shard_map/all_gather | solution.py:73
  61.4 42.1 %multiply_reduce_fusion.1 = (f32[1056]{0:T(1024)S(1)}, f32[1056,1024]{1,0:T(8,128)}) fusion(f32[1024]{0:T(1024)S(1)} %bitcast.27, bf16[1,1,1024,1024]{3,2,1,0:T(8,128)(2,1)} %all-gather.10.cloned.1.call-done, f32[1072,1024]{1,0:T(8,128)} %fusion.59, f32[1056]{0:T(1024)S(1)} %maximum_convert_fusion.2, f32[]{:T(128)S(6)} %mul.631, f32[]{:T(128)S(6)} %mul.628, ...), kind=kOutput, calls=%fused_computation.40 | convolution fusion | flops 2257845248 | bytes 79966528 | tf_op jit(solution)/shard_map/tgc,gcd->tgd/dot_general | solution.py:70
  103.5 0.3 dynamic-update-slice.1
  103.9 10.8 %all-reduce.1 = f32[4224]{0:T(1024)S(1)} all-reduce(f32[4224]{0:T(1024)S(1)} %dynamic-update-slice.1), channel_id=4, replica_groups=mesh['sp'=8,'tp'=4] {'tp'}, use_global_device_ids=true, to_apply=%add.1 | all-reduce | flops 4224 | bytes 33792
  114.8 4.7 %fusion.60 = f32[1056,1024]{1,0:T(8,128)} fusion(f32[1056,1024]{1,0:T(8,128)} %get-tuple-element.17, f32[1024]{0:T(1024)S(1)} %bitcast.23, f32[1056]{0:T(1024)S(1)} %add_rsqrt_fusion.1, pred[1056]{0:T(1024)(128)(4,1)S(1)} %compare_and_fusion.1), kind=kLoop, calls=%fused_computation.116 | loop fusion | flops 5406720 | bytes 8660128 | tf_op jit(solution)/shard_map/convert_element_type | solution.py:25
  119.6 41.5 %multiply_reduce_fusion.2 = (f32[1040]{0:T(1024)S(1)}, f32[1040,1024]{1,0:T(8,128)}) fusion(f32[1024]{0:T(1024)S(1)} %bitcast.26, bf16[1,1,1024,1024]{3,2,1,0:T(8,128)(2,1)} %all-gather.12.cloned.1.call-done, f32[1056,1024]{1,0:T(8,128)} %fusion.60, f32[1040]{0:T(1024)S(1)} %maximum_convert_fusion.1, f32[]{:T(128)S(6)} %mul.631, f32[]{:T(128)S(6)} %mul.628, ...), kind=kOutput, calls=%fused_computation.75 | convolution fusion | flops 2223635456 | bytes 78786752 | tf_op jit(solution)/shard_map/tgc,gcd->tgd/dot_general | solution.py:70
  161.1 0.3 dynamic-update-slice.2
  161.4 10.3 %all-reduce.2 = f32[4160]{0:T(1024)S(1)} all-reduce(f32[4160]{0:T(1024)S(1)} %dynamic-update-slice.2), channel_id=6, replica_groups=mesh['sp'=8,'tp'=4] {'tp'}, use_global_device_ids=true, to_apply=%add.2 | all-reduce | flops 4160 | bytes 33280
  171.8 4.7 %fusion.63 = f32[1040,1024]{1,0:T(8,128)} fusion(f32[1040,1024]{1,0:T(8,128)} %get-tuple-element.19, f32[1024]{0:T(1024)S(1)} %bitcast.22, f32[1040]{0:T(1024)S(1)} %add_rsqrt_fusion, pred[1040]{0:T(1024)(128)(4,1)S(1)} %compare_and_fusion), kind=kLoop, calls=%fused_computation.118 | loop fusion | flops 5324800 | bytes 8528976 | tf_op jit(solution)/shard_map/convert_element_type | solution.py:25
  176.5 39.4 %fusion.55 = bf16[1024,1024]{1,0:T(8,128)(2,1)} fusion(f32[1040,1024]{1,0:T(8,128)} %get-tuple-element.19, bf16[1,1,1024,1024]{3,2,1,0:T(8,128)(2,1)} %all-gather.14.cloned.1.call-done, f32[1024]{0:T(1024)S(1)} %bitcast.25, f32[1040,1024]{1,0:T(8,128)} %fusion.63, f32[1024]{0:T(1024)S(1)} %maximum_convert_fusion.3, f32[]{:T(128)S(6)} %mul.631, ...), kind=kOutput, calls=%fused_computation.110 | convolution fusion | flops 2186280960 | bytes 75505728 | tf_op jit(solution)/shard_map/tgc,gcd->tgd/dot_general | solution.py:70
  (31 shorter events, 0.7 us)
Async XLA Ops:
  6.5 15.5 %copy-start = (bf16[1024,1024]{1,0:T(8,128)(2,1)S(1)}, bf16[1024,1024]{1,0:T(8,128)(2,1)}, u32[]{:S(2)}) copy-start(bf16[1024,1024]{1,0:T(8,128)(2,1)} %param.4) | copy-start | bytes 6291460
  6.5 54.9 %all-gather.10.cloned.1.call-start = ((), (), s32[]{:S(2)}) async-start(), calls=%async_computation | async-start | bytes 2359296 | tf_op jit(solution)/shard_map/all_gather | solution.py:73
  8.7 110.8 %all-gather.12.cloned.1.call-start = ((), (), s32[]{:S(2)}) async-start(), calls=%async_computation.1 | async-start | bytes 2359296 | tf_op jit(solution)/shard_map/all_gather | solution.py:73
  9.5 167.0 %all-gather.14.cloned.1.call-start = ((), (), s32[]{:S(2)}) async-start(), calls=%async_computation.2 | async-start | bytes 2359296 | tf_op jit(solution)/shard_map/all_gather | solution.py:73
  10.4 11.7 %collective-permute-start = (bf16[24,1024]{1,0:T(8,128)(2,1)S(1)}, bf16[24,1024]{1,0:T(8,128)(2,1)S(1)}, u32[]{:S(2)}, u32[]{:S(2)}) collective-permute-start(bf16[24,1024]{1,0:T(8,128)(2,1)S(1)} %get-tuple-element.5), channel_id=1, source_target_pairs={{0,4},{4,8},{8,12},{12,16},{16,20},{20,24},{24,28},{1,5},{5,9},{9,... | collective-permute-start | bytes 147464 | tf_op jit(solution)/shard_map/ppermute | solution.py:18
  15.3 6.8 %collective-permute-start.1 = (bf16[24,1024]{1,0:T(8,128)(2,1)S(1)}, bf16[24,1024]{1,0:T(8,128)(2,1)S(1)}, u32[]{:S(2)}, u32[]{:S(2)}) collective-permute-start(bf16[24,1024]{1,0:T(8,128)(2,1)S(1)} %get-tuple-element.6), channel_id=1, source_target_pairs={{4,0},{8,4},{12,8},{16,12},{20,16},{24,20},{28,24},{5,1},{9,5},{13... | collective-permute-start | bytes 147464 | tf_op jit(solution)/shard_map/ppermute | solution.py:19
Sparse Core Ops, SparseCore 0:
  9.5 51.8 all-gather.9
  63.5 47.5 all-gather.11
  113.3 47.6 all-gather.13
